TPU v7x, 32 devices: a whole 2x2x4 slice. The times are simulated.
32 devices in a mesh: fs: 4 (over y, x), tp: 8 (over z, core).
Axes of the slice: x: 2, y: 2, z: 4, core: 2. Of those that a mesh axis runs over, the one named last changes fastest.
Arguments:
- inputs: bfloat16 [8, 320, 2048], P('tp'), may hold values from -6 to 6
- cotangent: bfloat16 [8, 320, 2048], P('tp'), may hold values from -8 to 8
- gate_weight: bfloat16 [2048, 5632], P('tp', 'fs'), may hold values from -0.125 to 0.125
- up_weight: bfloat16 [2048, 5632], P('tp', 'fs'), may hold values from -0.125 to 0.125
- down_weight: bfloat16 [5632, 2048], P('fs', 'tp'), may hold values from -0.078125 to 0.078125
Outputs:
- input_grad: bfloat16 [8, 320, 2048], P('tp')
- down_grad: float32 [5632, 2048], P('fs', 'tp')
All inputs are finite; a program needn't handle non-finite values.
Results may differ from a plain program's by a relative error of at most 0.023.
Values may be sent and summed in bfloat16 or wider, within the bound.
A program may use at most 64 MiB of HBM per device.

v0:
```python
import jax
import jax.numpy as jnp
from jax import lax
from jax.sharding import PartitionSpec as P


def contract_hidden(left, right):
    return lax.dot_general(
        left, right, (((1,), (1,)), ((), ())), preferred_element_type=jnp.float32
    )


def contract_tokens(left, right):
    return lax.dot_general(
        left, right, (((0,), (0,)), ((), ())), preferred_element_type=jnp.float32
    )


def per_device(inputs, cotangent, gate_weight, up_weight, down_weight):
    rows_in = inputs[0]
    rows_grad = cotangent[0]
    token_count = rows_in.shape[0]
    model_width = rows_in.shape[1]
    gate_full, up_full, down_tall = (
        lax.all_gather(gate_weight, "tp", axis=0, tiled=True),
        lax.all_gather(up_weight, "tp", axis=0, tiled=True),
        lax.all_gather(down_weight.T, "tp", axis=0, tiled=True),
    )
    gate_pre = jnp.dot(rows_in, gate_full, preferred_element_type=jnp.float32)
    up_pre = jnp.dot(rows_in, up_full, preferred_element_type=jnp.float32)
    sig = jax.nn.sigmoid(gate_pre)
    hidden = (gate_pre * sig * up_pre).astype(jnp.bfloat16)
    hidden_grad = jnp.dot(rows_grad, down_tall, preferred_element_type=jnp.float32)
    gate_grad = (hidden_grad * up_pre * sig * (1.0 + gate_pre * (1.0 - sig))).astype(jnp.bfloat16)
    up_grad = (hidden_grad * gate_pre * sig).astype(jnp.bfloat16)
    partial_down = contract_tokens(hidden, rows_grad)
    down_grad = lax.psum_scatter(
        partial_down.astype(jnp.bfloat16), "tp", scatter_dimension=1, tiled=True
    ).astype(jnp.float32)
    own_sum = lax.psum_scatter(
        (contract_hidden(gate_grad, gate_full) + contract_hidden(up_grad, up_full)).astype(
            jnp.bfloat16
        ),
        "fs",
        scatter_dimension=0,
        tiled=True,
    )
    whole_grad = lax.all_gather(own_sum, "fs", axis=0, tiled=True)
    input_grad = whole_grad.reshape(1, token_count, model_width)
    return (input_grad, down_grad)


def solution(mesh):
    return jax.shard_map(
        per_device,
        mesh=mesh,
        in_specs=(
            P("tp", None, None),
            P("tp", None, None),
            P("tp", "fs"),
            P("tp", "fs"),
            P("fs", "tp"),
        ),
        out_specs=(P("tp", None, None), P("fs", "tp")),
        check_vma=False,
    )
```

profile of v0, /device:TPU:0, one launch (start us, length us, event | category | flops | bytes accessed | tf_op | source)
XLA Modules:
  0.0 342.6 jit_solution(16475560544088254756)
XLA Ops:
  7.2 0.0 copy-start
  7.2 0.0 copy-start.3
  7.2 0.0 all-gather.9.cloned.1.call-start
  7.2 0.7 all-gather.9.cloned.1.call-update
  7.9 0.0 all-gather.7.cloned.1.call-start
  8.0 0.7 all-gather.7.cloned.1.call-update
  8.7 0.0 all-gather.5.cloned.1.call-start
  8.7 0.7 all-gather.5.cloned.1.call-update
  9.4 0.0 reduce-scatter.3.cloned.1.call-start
  9.5 63.3 %all-gather.9.cloned.1.call-done = bf16[2048,1408]{1,0:T(8,128)(2,1)} async-done(((bf16[256,1408]{1,0:T(8,128)(2,1)}), bf16[2048,1408]{1,0:T(8,128)(2,1)}) %all-gather.9.cloned.1.call-update) | async-done | bytes 5767184 | tf_op jit(solution)/shard_map/all_gather | solution.py:25
  72.8 0.0 copy-done.3
  72.8 6.1 %fusion.1 = f32[320,1408]{1,0:T(8,128)} fusion(bf16[2048,1408]{1,0:T(8,128)(2,1)} %all-gather.9.cloned.1.call-done, bf16[1,320,2048]{2,1,0:T(8,128)(2,1)S(1)} %copy-done.3), kind=kOutput, calls=%fused_computation.7 | convolution fusion | flops 1845493760 | bytes 8880128 | tf_op jit(solution)/shard_map/dot_general | solution.py:29
  78.8 54.6 %all-gather.7.cloned.1.call-done = bf16[2048,1408]{1,0:T(8,128)(2,1)} async-done(((bf16[256,1408]{1,0:T(8,128)(2,1)}), bf16[2048,1408]{1,0:T(8,128)(2,1)}) %all-gather.7.cloned.1.call-update) | async-done | bytes 5767184 | tf_op jit(solution)/shard_map/all_gather | solution.py:26
  133.5 6.1 %fusion.3 = f32[320,1408]{1,0:T(8,128)} fusion(bf16[2048,1408]{1,0:T(8,128)(2,1)} %all-gather.7.cloned.1.call-done, bf16[1,320,2048]{2,1,0:T(8,128)(2,1)S(1)} %copy-done.3), kind=kOutput, calls=%fused_computation.9 | convolution fusion | flops 1845493760 | bytes 8880128 | tf_op jit(solution)/shard_map/dot_general | solution.py:30
  139.6 0.0 copy-start.4
  139.6 55.0 %all-gather.5.cloned.1.call-done = bf16[2048,1408]{0,1:T(8,128)(2,1)} async-done(((bf16[256,1408]{0,1:T(8,128)(2,1)}), bf16[2048,1408]{0,1:T(8,128)(2,1)}) %all-gather.5.cloned.1.call-update) | async-done | bytes 5767184 | tf_op jit(solution)/shard_map/all_gather | solution.py:27
  194.6 0.0 copy-done
  194.6 0.0 copy-start.2
  194.6 0.0 slice-start
  194.6 5.0 %fusion.6 = f32[320,1408]{1,0:T(8,128)S(1)} fusion(bf16[2048,1408]{0,1:T(8,128)(2,1)} %all-gather.5.cloned.1.call-done, bf16[1,320,2048]{2,1,0:T(8,128)(2,1)S(1)} %copy-done), kind=kOutput, calls=%fused_computation.12 | convolution fusion | flops 1845493760 | bytes 8880128 | tf_op jit(solution)/shard_map/dot_general | solution.py:33
  199.6 0.0 copy-done.4
  199.6 0.0 copy-done.2
  199.6 0.0 slice-start.1
  199.6 4.1 %fusion.8 = f32[320,2048]{1,0:T(8,128)S(1)} fusion(bf16[2048,1408]{1,0:T(8,128)(2,1)S(1)} %copy-done.2, f32[320,1408]{1,0:T(8,128)S(1)} %copy-done.4, f32[320,1408]{1,0:T(8,128)S(1)} %fusion.6, f32[320,1408]{1,0:T(8,128)} %fusion.3), kind=kOutput, calls=%fused_computation.14 | convolution fusion | flops 1849999360 | bytes 13795328 | tf_op jit(solution)/shard_map/dot_general | solution.py:8
  203.8 0.0 slice-done
  203.8 0.0 slice-done.1
  203.8 3.4 fusion
  207.2 0.0 reduce-scatter.3.cloned.1.call-update
  207.2 0.0 all-gather.11.cloned.1.call-start
  207.3 27.8 %reduce-scatter.3.cloned.1.call-done = bf16[80,2048]{1,0:T(8,128)(2,1)} async-done(((bf16[320,2048]{1,0:T(8,128)(2,1)}), bf16[80,2048]{1,0:T(8,128)(2,1)}) %reduce-scatter.3.cloned.1.call-update) | async-done | bytes 327696 | tf_op jit(solution)/shard_map/reduce_scatter | solution.py:40
  235.0 0.0 all-gather.11.cloned.1.call-update
  235.1 0.0 reduce-scatter.5.cloned.1.call-start
  235.1 6.7 %convolution_convert_fusion = bf16[1408,2048]{1,0:T(8,128)(2,1)} fusion(bf16[1,320,2048]{2,1,0:T(8,128)(2,1)S(1)} %copy-done, f32[320,1408]{1,0:T(8,128)} %fusion.3, f32[320,1408]{1,0:T(8,128)S(1)} %copy-done.4), kind=kOutput, calls=%fused_computation | convolution fusion | flops 1851080704 | bytes 10682368 | tf_op jit(solution)/shard_map/dot_general | solution.py:14
  241.8 0.0 reduce-scatter.5.cloned.1.call-update
  241.8 23.6 %all-gather.11.cloned.1.call-done = bf16[320,2048]{1,0:T(8,128)(2,1)} async-done(((bf16[80,2048]{1,0:T(8,128)(2,1)}), bf16[320,2048]{1,0:T(8,128)(2,1)}) %all-gather.11.cloned.1.call-update) | async-done | bytes 1310736 | tf_op jit(solution)/shard_map/all_gather | solution.py:48
  265.4 0.0 copy-start.1
  265.4 67.0 %reduce-scatter.5.cloned.1.call-done = bf16[1408,256]{1,0:T(8,128)(2,1)} async-done(((bf16[1408,2048]{1,0:T(8,128)(2,1)}), bf16[1408,256]{1,0:T(8,128)(2,1)}) %reduce-scatter.5.cloned.1.call-update) | async-done | bytes 720912 | tf_op jit(solution)/shard_map/reduce_scatter | solution.py:37
  332.4 2.3 convert_element_type.23
  334.7 0.0 copy-done.1
  334.7 1.1 copy.8
  (1 shorter events, 0.0 us)
Async XLA Ops:
  7.2 187.4 %copy-start = (bf16[1,320,2048]{2,1,0:T(8,128)(2,1)S(1)}, bf16[1,320,2048]{2,1,0:T(8,128)(2,1)}, u32[]{:S(2)}) copy-start(bf16[1,320,2048]{2,1,0:T(8,128)(2,1)} %param.6) | copy-start | bytes 3932164
  7.2 65.6 %copy-start.3 = (bf16[1,320,2048]{2,1,0:T(8,128)(2,1)S(1)}, bf16[1,320,2048]{2,1,0:T(8,128)(2,1)}, u32[]{:S(2)}) copy-start(bf16[1,320,2048]{2,1,0:T(8,128)(2,1)} %param.5) | copy-start | bytes 3932164
  7.2 65.6 %all-gather.9.cloned.1.call-start = ((), (), s32[]{:S(2)}) async-start(), calls=%async_computation.4 | async-start | bytes 6488064 | tf_op jit(solution)/shard_map/all_gather | solution.py:25
  7.9 125.5 %all-gather.7.cloned.1.call-start = ((), (), s32[]{:S(2)}) async-start(), calls=%async_computation.3 | async-start | bytes 6488064 | tf_op jit(solution)/shard_map/all_gather | solution.py:26
  8.7 185.9 %all-gather.5.cloned.1.call-start = ((), (), s32[]{:S(2)}) async-start(), calls=%async_computation.2 | async-start | bytes 6488064 | tf_op jit(solution)/shard_map/all_gather | solution.py:27
  9.4 225.6 %reduce-scatter.3.cloned.1.call-start = ((), (), s32[]{:S(2)}) async-start(), calls=%async_computation.5 | async-start | bytes 1638400 | tf_op jit(solution)/shard_map/reduce_scatter | solution.py:40
  139.6 60.1 %copy-start.4 = (f32[320,1408]{1,0:T(8,128)S(1)}, f32[320,1408]{1,0:T(8,128)}, u32[]{:S(2)}) copy-start(f32[320,1408]{1,0:T(8,128)} %fusion.1) | copy-start | bytes 5406724
  194.6 5.0 %copy-start.2 = (bf16[2048,1408]{1,0:T(8,128)(2,1)S(1)}, bf16[2048,1408]{1,0:T(8,128)(2,1)}, u32[]{:S(2)}) copy-start(bf16[2048,1408]{1,0:T(8,128)(2,1)} %all-gather.9.cloned.1.call-done) | copy-start | bytes 17301508
  194.6 9.2 %slice-start = ((s8[5767168]{0:T(1024)(128)(4,1)}), s8[4194304]{0:T(1024)(128)(4,1)S(1)}, s32[]{:S(2)}) async-start(s8[5767168]{0:T(1024)(128)(4,1)} %bitcast.19), calls=%async_computation.8 | async-start | bytes 8388608
  199.6 4.2 %slice-start.1 = ((s8[5767168]{0:T(1024)(128)(4,1)}), s8[1572864]{0:T(1024)(128)(4,1)S(1)}, s32[]{:S(2)}) async-start(s8[5767168]{0:T(1024)(128)(4,1)} %bitcast.19), calls=%async_computation.9 | async-start | bytes 3145728
  207.2 58.2 %all-gather.11.cloned.1.call-start = ((), (), s32[]{:S(2)}) async-start(), calls=%async_computation.6 | async-start | bytes 1638400 | tf_op jit(solution)/shard_map/all_gather | solution.py:48
  235.1 97.3 %reduce-scatter.5.cloned.1.call-start = ((), (), s32[]{:S(2)}) async-start(), calls=%async_computation.7 | async-start | bytes 6488064 | tf_op jit(solution)/shard_map/reduce_scatter | solution.py:37
  265.4 69.3 %copy-start.1 = (bf16[320,2048]{1,0:T(8,128)(2,1)S(1)}, bf16[320,2048]{1,0:T(8,128)(2,1)}, u32[]{:S(2)}) copy-start(bf16[320,2048]{1,0:T(8,128)(2,1)} %all-gather.11.cloned.1.call-done) | copy-start | bytes 3932164
Sparse Core Ops, SparseCore 0:
  9.6 63.0 all-gather.8
  74.4 59.0 all-gather.6
  135.1 59.4 all-gather.4
  207.3 27.6 reduce-scatter.2
  236.7 28.6 all-gather.10
  267.6 64.7 reduce-scatter.4
where the time goes:
time: 343 us
  waiting for transfers between devices  293 us (85%)
  matrix products  31.3 us (9%)
  between operations  14.2 us (4%)
    reduce_scatter x1, waiting for transfers between devices, per_device(): lax.psum_scatter(partial_down.astype(jnp.bfloat16), 'tp', scatter_dimensi...  67 us
    all_gather x1, waiting for transfers between devices, per_device(): lax.all_gather(gate_weight, 'tp', axis=0, tiled=True)  63.3 us
    all_gather x1, waiting for transfers between devices, per_device(): lax.all_gather(down_weight.T, 'tp', axis=0, tiled=True)  55 us
    all_gather x1, waiting for transfers between devices, per_device(): lax.all_gather(up_weight, 'tp', axis=0, tiled=True)  54.6 us
    reduce_scatter x1, waiting for transfers between devices, per_device(): lax.psum_scatter((contract_hidden(gate_grad, gate_full) + contract_hidden...  27.8 us
    all_gather x1, waiting for transfers between devices, per_device(): whole_grad = lax.all_gather(own_sum, 'fs', axis=0, tiled=True)  23.6 us
    dot_general x2, matrix products, contract_hidden(): lax.dot_general(left, right, (((1,), (1,)), ((), ())), preferred_element_...  7.51 us
  transfers between devices with their start and end apart: 6, of which 6 were waited for; matrix products, arithmetic and copies ran while one was open for 5% of the time, Pallas kernels for 0%

commit v1 on v0

--- a/solution.py
+++ b/solution.py
@@ -2,6 +2,13 @@
 import jax.numpy as jnp
 from jax import lax
 from jax.sharding import PartitionSpec as P
+
+
+def all_by_exchange(x, name, d):
+    count = lax.axis_size(name)
+    blocks = jnp.stack([x for _ in range(count)])
+    blocks = lax.all_to_all(blocks, name, split_axis=0, concat_axis=0)
+    return jnp.concatenate(blocks, axis=d)
 
 
 def contract_hidden(left, right):
@@ -23,7 +30,7 @@
     model_width = rows_in.shape[1]
     gate_full, up_full, down_tall = (
         lax.all_gather(gate_weight, "tp", axis=0, tiled=True),
-        lax.all_gather(up_weight, "tp", axis=0, tiled=True),
+        all_by_exchange(up_weight, "tp", 0),
         lax.all_gather(down_weight.T, "tp", axis=0, tiled=True),
     )
     gate_pre = jnp.dot(rows_in, gate_full, preferred_element_type=jnp.float32)

time: 343 us -> 401 us (1.17)
  waiting for transfers between devices: 293 us -> 340 us
  starting transfers between devices: 0.23 us -> 6.68 us
  local copies, waits for them, and re-layouts: 1.09 us -> 5.43 us
    all_to_all x0 -> x1, waiting for transfers between devices: none -> 220 us  [all_by_exchange(): blocks = lax.all_to_all(blocks, name, split_axis=0, concat_axis=0)]
    all_gather x1, waiting for transfers between devices: 63.3 us -> 0.01 us  [per_device(): lax.all_gather(gate_weight, 'tp', axis=0, tiled=True)]
    all_gather x1, waiting for transfers between devices: 55 us -> 0.01 us  [per_device(): lax.all_gather(down_weight.T, 'tp', axis=0, tiled=True)]
    all_gather x1 -> x0, waiting for transfers between devices: 54.6 us -> none  [per_device(): lax.all_gather(up_weight, 'tp', axis=0, tiled=True)]
    all_to_all x0 -> x1, starting transfers between devices: none -> 6.49 us  [all_by_exchange(): blocks = lax.all_to_all(blocks, name, split_axis=0, concat_axis=0)]
    another operation x0 -> x1, local copies, waits for them, and re-layouts: none -> 4.03 us  [all_by_exchange(): blocks = jnp.stack([x for _ in range(count)])]
  transfers between devices with their start and end apart: 6 -> 6, of which waited for: 6 -> 4; matrix products, arithmetic and copies ran while one was open for 5% -> 6% of each run, Pallas kernels for 0% -> 0%
where the time goes in v1:
time: 401 us
  waiting for transfers between devices  340 us (85%)
  matrix products  32.3 us (8%)
  between operations  13.8 us (3%)
  starting transfers between devices  6.68 us (2%)
  local copies, waits for them, and re-layouts  5.43 us (1%)
    all_to_all x1, waiting for transfers between devices, all_by_exchange(): blocks = lax.all_to_all(blocks, name, split_axis=0, concat_axis=0)  220 us
    reduce_scatter x1, waiting for transfers between devices, per_device(): lax.psum_scatter(partial_down.astype(jnp.bfloat16), 'tp', scatter_dimensi...  66.9 us
    reduce_scatter x1, waiting for transfers between devices, per_device(): lax.psum_scatter((contract_hidden(gate_grad, gate_full) + contract_hidden...  28.5 us
    all_gather x1, waiting for transfers between devices, per_device(): whole_grad = lax.all_gather(own_sum, 'fs', axis=0, tiled=True)  23.6 us
    dot_general x2, matrix products, contract_hidden(): lax.dot_general(left, right, (((1,), (1,)), ((), ())), preferred_element_...  8.49 us
  transfers between devices with their start and end apart: 6, of which 4 were waited for; matrix products, arithmetic and copies ran while one was open for 6% of the time, Pallas kernels for 0%

profile of v1, /device:TPU:0, one launch (start us, length us, event | category | flops | bytes accessed | tf_op | source)
XLA Modules:
  0.0 400.8 jit_solution(15408034538986337210)
XLA Ops:
  7.2 0.0 copy-start
  7.2 0.0 all-gather.6.cloned.1.call-start
  7.2 0.7 all-gather.6.cloned.1.call-update
  7.9 4.0 %stack.2 = bf16[8,256,1408]{2,1,0:T(8,128)(2,1)} broadcast(bf16[256,1408]{1,0:T(8,128)(2,1)} %param.8), dimensions={1,2} | broadcast | bytes 6488064 | tf_op jit(solution)/shard_map/stack | solution.py:9
  11.9 0.0 copy-start.3
  11.9 6.5 %all-to-all-start = ((bf16[8,256,1408]{2,1,0:T(8,128)(2,1)}), bf16[8,256,1408]{2,1,0:T(8,128)(2,1)}, u32[]{:S(2)}, u32[]{:S(2)}) async-start(bf16[8,256,1408]{2,1,0:T(8,128)(2,1)} %stack.2), calls=%async_computation | async-start | bytes 11534336 | tf_op jit(solution)/shard_map/all_to_all | solution.py:10
  18.4 0.0 all-gather.4.cloned.1.call-start
  18.5 0.7 all-gather.4.cloned.1.call-update
  19.2 0.0 reduce-scatter.3.cloned.1.call-start
  19.2 219.7 %all-to-all-done = bf16[8,256,1408]{2,1,0:T(8,128)(2,1)} async-done(((bf16[8,256,1408]{2,1,0:T(8,128)(2,1)}), bf16[8,256,1408]{2,1,0:T(8,128)(2,1)}, u32[]{:S(2)}, u32[]{:S(2)}) %all-to-all-start) | async-done | bytes 5767200 | tf_op jit(solution)/shard_map/all_to_all | solution.py:10
  238.9 0.0 copy-done.3
  238.9 6.1 %fusion.3 = f32[320,1408]{1,0:T(8,128)} fusion(bf16[2048,1408]{1,0:T(8,128)(2,1)} %bitcast.3, bf16[1,320,2048]{2,1,0:T(8,128)(2,1)S(1)} %copy-done.3), kind=kOutput, calls=%fused_computation.9 | convolution fusion | flops 1845493760 | bytes 8880128 | tf_op jit(solution)/shard_map/dot_general | solution.py:37
  245.0 0.0 all-gather.6.cloned.1.call-done
  245.0 6.0 %fusion.1 = f32[320,1408]{1,0:T(8,128)} fusion(bf16[2048,1408]{1,0:T(8,128)(2,1)} %all-gather.6.cloned.1.call-done, bf16[1,320,2048]{2,1,0:T(8,128)(2,1)S(1)} %copy-done.3), kind=kOutput, calls=%fused_computation.7 | convolution fusion | flops 1845493760 | bytes 8880128 | tf_op jit(solution)/shard_map/dot_general | solution.py:36
  251.1 0.0 copy-start.4
  251.1 0.0 all-gather.4.cloned.1.call-done
  251.1 0.0 copy-done
  251.1 0.0 copy-start.2
  251.1 0.0 copy-start.5
  251.1 5.0 %fusion.6 = f32[320,1408]{1,0:T(8,128)S(1)} fusion(bf16[2048,1408]{0,1:T(8,128)(2,1)} %all-gather.4.cloned.1.call-done, bf16[1,320,2048]{2,1,0:T(8,128)(2,1)S(1)} %copy-done), kind=kOutput, calls=%fused_computation.12 | convolution fusion | flops 1845493760 | bytes 8880128 | tf_op jit(solution)/shard_map/dot_general | solution.py:40
  256.1 0.0 copy-done.4
  256.1 0.0 copy-done.2
  256.1 0.3 copy-done.5
  256.4 2.5 fusion.8
  258.9 6.0 %fusion = bf16[320,2048]{1,0:T(8,128)(2,1)} fusion(f32[320,2048]{1,0:T(8,128)S(1)} %fusion.8, bf16[2048,1408]{1,0:T(8,128)(2,1)} %bitcast.3, f32[320,1408]{1,0:T(8,128)S(1)} %fusion.6, f32[320,1408]{1,0:T(8,128)S(1)} %copy-done.4), kind=kOutput, calls=%fused_computation.2 | convolution fusion | flops 1849507840 | bytes 13303808 | tf_op jit(solution)/shard_map/dot_general | solution.py:15
  264.9 0.0 reduce-scatter.3.cloned.1.call-update
  264.9 0.0 all-gather.8.cloned.1.call-start
  265.0 28.5 %reduce-scatter.3.cloned.1.call-done = bf16[80,2048]{1,0:T(8,128)(2,1)} async-done(((bf16[320,2048]{1,0:T(8,128)(2,1)}), bf16[80,2048]{1,0:T(8,128)(2,1)}) %reduce-scatter.3.cloned.1.call-update) | async-done | bytes 327696 | tf_op jit(solution)/shard_map/reduce_scatter | solution.py:47
  293.5 0.0 all-gather.8.cloned.1.call-update
  293.5 0.0 reduce-scatter.5.cloned.1.call-start
  293.6 6.7 %convolution_convert_fusion = bf16[1408,2048]{1,0:T(8,128)(2,1)} fusion(bf16[1,320,2048]{2,1,0:T(8,128)(2,1)S(1)} %copy-done, f32[320,1408]{1,0:T(8,128)} %fusion.3, f32[320,1408]{1,0:T(8,128)S(1)} %copy-done.4), kind=kOutput, calls=%fused_computation | convolution fusion | flops 1851080704 | bytes 10682368 | tf_op jit(solution)/shard_map/dot_general | solution.py:21
  300.3 0.0 reduce-scatter.5.cloned.1.call-update
  300.3 23.6 %all-gather.8.cloned.1.call-done = bf16[320,2048]{1,0:T(8,128)(2,1)} async-done(((bf16[80,2048]{1,0:T(8,128)(2,1)}), bf16[320,2048]{1,0:T(8,128)(2,1)}) %all-gather.8.cloned.1.call-update) | async-done | bytes 1310736 | tf_op jit(solution)/shard_map/all_gather | solution.py:55
  323.9 0.0 copy-start.1
  323.9 66.9 %reduce-scatter.5.cloned.1.call-done = bf16[1408,256]{1,0:T(8,128)(2,1)} async-done(((bf16[1408,2048]{1,0:T(8,128)(2,1)}), bf16[1408,256]{1,0:T(8,128)(2,1)}) %reduce-scatter.5.cloned.1.call-update) | async-done | bytes 720912 | tf_op jit(solution)/shard_map/reduce_scatter | solution.py:44
  390.9 2.3 convert_element_type.23
  393.2 0.0 copy-done.1
  393.2 1.1 copy.8
Async XLA Ops:
  7.2 243.9 %copy-start = (bf16[1,320,2048]{2,1,0:T(8,128)(2,1)S(1)}, bf16[1,320,2048]{2,1,0:T(8,128)(2,1)}, u32[]{:S(2)}) copy-start(bf16[1,320,2048]{2,1,0:T(8,128)(2,1)} %param.6) | copy-start | bytes 3932164
  7.2 237.8 %all-gather.6.cloned.1.call-start = ((), (), s32[]{:S(2)}) async-start(), calls=%async_computation.4 | async-start | bytes 6488064 | tf_op jit(solution)/shard_map/all_gather | solution.py:32
  11.9 227.0 %copy-start.3 = (bf16[1,320,2048]{2,1,0:T(8,128)(2,1)S(1)}, bf16[1,320,2048]{2,1,0:T(8,128)(2,1)}, u32[]{:S(2)}) copy-start(bf16[1,320,2048]{2,1,0:T(8,128)(2,1)} %param.5) | copy-start | bytes 3932164
  11.9 227.0 %all-to-all-start = ((bf16[8,256,1408]{2,1,0:T(8,128)(2,1)}), bf16[8,256,1408]{2,1,0:T(8,128)(2,1)}, u32[]{:S(2)}, u32[]{:S(2)}) async-start(bf16[8,256,1408]{2,1,0:T(8,128)(2,1)} %stack.2), calls=%async_computation | async-start | bytes 11534336 | tf_op jit(solution)/shard_map/all_to_all | solution.py:10
  18.4 232.6 %all-gather.4.cloned.1.call-start = ((), (), s32[]{:S(2)}) async-start(), calls=%async_computation.3 | async-start | bytes 6488064 | tf_op jit(solution)/shard_map/all_gather | solution.py:34
  19.2 274.3 %reduce-scatter.3.cloned.1.call-start = ((), (), s32[]{:S(2)}) async-start(), calls=%async_computation.5 | async-start | bytes 1638400 | tf_op jit(solution)/shard_map/reduce_scatter | solution.py:47
  251.1 5.0 %copy-start.4 = (f32[320,1408]{1,0:T(8,128)S(1)}, f32[320,1408]{1,0:T(8,128)}, u32[]{:S(2)}) copy-start(f32[320,1408]{1,0:T(8,128)} %fusion.1) | copy-start | bytes 5406724
  251.1 5.0 %copy-start.2 = (bf16[2048,1408]{1,0:T(8,128)(2,1)S(1)}, bf16[2048,1408]{1,0:T(8,128)(2,1)}, u32[]{:S(2)}) copy-start(bf16[2048,1408]{1,0:T(8,128)(2,1)} %all-gather.6.cloned.1.call-done) | copy-start | bytes 17301508
  251.1 5.4 %copy-start.5 = (f32[320,1408]{1,0:T(8,128)S(1)}, f32[320,1408]{1,0:T(8,128)}, u32[]{:S(2)}) copy-start(f32[320,1408]{1,0:T(8,128)} %fusion.3) | copy-start | bytes 5406724
  264.9 59.0 %all-gather.8.cloned.1.call-start = ((), (), s32[]{:S(2)}) async-start(), calls=%async_computation.6 | async-start | bytes 1638400 | tf_op jit(solution)/shard_map/all_gather | solution.py:55
  293.5 97.3 %reduce-scatter.5.cloned.1.call-start = ((), (), s32[]{:S(2)}) async-start(), calls=%async_computation.7 | async-start | bytes 6488064 | tf_op jit(solution)/shard_map/reduce_scatter | solution.py:44
  323.9 69.3 %copy-start.1 = (bf16[320,2048]{1,0:T(8,128)(2,1)S(1)}, bf16[320,2048]{1,0:T(8,128)(2,1)}, u32[]{:S(2)}) copy-start(bf16[320,2048]{1,0:T(8,128)(2,1)} %all-gather.8.cloned.1.call-done) | copy-start | bytes 3932164
Sparse Core Ops, SparseCore 0:
  9.6 108.3 all-gather.5
  119.6 114.3 all-gather.3
  265.1 28.3 reduce-scatter.2
  295.2 28.6 all-gather.7
  326.1 64.7 reduce-scatter.4
